TPU v7x, 32 devices: a whole 2x2x4 slice. The times are simulated.
32 devices in a mesh: fs: 2 (over core), tp: 16 (over z, y, x).
Axes of the slice: x: 2, y: 2, z: 4, core: 2. Of those that a mesh axis runs over, the one named last changes fastest.
Arguments:
- trained_gate: float32 [16, 504, 2048], P(None, 'fs', 'tp'), may hold values from -0.125 to 0.125
- trained_up: float32 [16, 504, 2048], P(None, 'fs', 'tp'), may hold values from -0.125 to 0.125
- trained_down: float32 [16, 504, 2048], P(None, 'fs', 'tp'), may hold values from -0.25 to 0.25
- trained_shared_gate: float32 [504, 2048], P('fs', 'tp'), may hold values from -0.125 to 0.125
- trained_shared_up: float32 [504, 2048], P('fs', 'tp'), may hold values from -0.125 to 0.125
- trained_shared_down: float32 [504, 2048], P('fs', 'tp'), may hold values from -0.25 to 0.25
- ffn_gain: float32 [2048], P('tp'), may hold values from 0.1 to 1.9
- prompt_tokens: bfloat16 [512, 2048], P('fs'), may hold values from -6 to 6
- expert_ids: int32 [512, 8], P('fs'), may hold values from 0 to 15, all different within a row; in each aligned block of 256 rows (0 to 255, 256 to 511, ...) at most 256 rows name the same one
- route_scores: float32 [512, 8], P('fs'), may hold values from 0.05 to 1
Outputs:
- served_gate: bfloat16 [16, 504, 2048], P('tp')
- served_up: bfloat16 [16, 504, 2048], P('tp')
- served_down: bfloat16 [16, 504, 2048], P('tp')
- served_shared_gate: bfloat16 [504, 2048], P(None, 'tp')
- served_shared_up: bfloat16 [504, 2048], P(None, 'tp')
- served_shared_down: bfloat16 [504, 2048], P(None, 'tp')
- mixture_out: bfloat16 [512, 2048], P('fs', 'tp')
Inputs may be any that keep to these rules, and one draw needn't show every extreme that they name: `expert_ids`: each row names 8 different experts, and every expert is named by some row. Within the 256 rows of one index of fs no expert is named by more than 256 rows, and in every draw some expert is named by exactly 256 rows of some index of fs.
All inputs are finite; a program needn't handle non-finite values.
Results may differ from a plain program's by a relative error of at most 0.0082.
Values may be sent and summed in bfloat16 or wider, within the bound.
No kernel may reach another device: no remote copies, remote signals or barrier semaphores. Data moves between devices by JAX's collectives and lax.ppermute only.
A program may use at most 64 MiB of HBM per device.

v0:
```python
import jax
import jax.numpy as jnp
from jax import lax
from jax.sharding import PartitionSpec as P

EPSILON = 1e-06
ROUTED_SCALE = 2.5


def contract(left, right):
    return lax.dot_general(
        left, right, (((1,), (1,)), ((), ())), preferred_element_type=jnp.float32
    )


def on_device(
    trained_gate,
    trained_up,
    trained_down,
    trained_shared_gate,
    trained_shared_up,
    trained_shared_down,
    ffn_gain,
    prompt_tokens,
    expert_ids,
    route_scores,
):
    gate_cast = (trained_gate * ffn_gain[None, None, :]).astype(jnp.bfloat16)
    up_cast = (trained_up * ffn_gain[None, None, :]).astype(jnp.bfloat16)
    down_cast = trained_down.astype(jnp.bfloat16)
    shared_gate_cast = (trained_shared_gate * ffn_gain[None, :]).astype(jnp.bfloat16)[None]
    shared_up_cast = (trained_shared_up * ffn_gain[None, :]).astype(jnp.bfloat16)[None]
    shared_down_cast = trained_shared_down.astype(jnp.bfloat16)[None]
    expert_gate, expert_up, expert_down = (
        lax.all_to_all(gate_cast, "tp", split_axis=0, concat_axis=2, tiled=True),
        lax.all_to_all(up_cast, "tp", split_axis=0, concat_axis=2, tiled=True),
        lax.all_to_all(down_cast, "tp", split_axis=0, concat_axis=2, tiled=True),
    )
    token_count, model_width = prompt_tokens.shape
    tokens_float = prompt_tokens.astype(jnp.float32)
    normed = (
        tokens_float
        * lax.rsqrt(jnp.mean(tokens_float * tokens_float, axis=1, keepdims=True) + EPSILON)
    ).astype(jnp.bfloat16)
    column_width = ffn_gain.shape[0]
    expert_index = lax.axis_index("tp")
    normed_cols = lax.dynamic_slice_in_dim(normed, expert_index * column_width, column_width, 1)
    expert_count = lax.axis_size("tp")
    top_count = expert_ids.shape[1]
    capacity = min(token_count, 5 * token_count * top_count // (2 * expert_count))
    route_weight = ROUTED_SCALE * route_scores / jnp.sum(route_scores, axis=1, keepdims=True)
    chosen = expert_ids == expert_index
    present = jnp.any(chosen, axis=1)
    position = jnp.cumsum(present.astype(jnp.int32)) - 1
    slot_match = (position[None, :] == jnp.arange(capacity, dtype=jnp.int32)[:, None]) & present[
        None, :
    ]
    slot_token = jnp.sum(
        jnp.where(slot_match, jnp.arange(token_count, dtype=jnp.int32)[None, :], 0), axis=1
    )
    slot_rows = jnp.take(normed, slot_token, axis=0)
    gathered = (
        lax.all_gather(expert_gate, "fs", axis=1, tiled=True),
        lax.all_gather(expert_up, "fs", axis=1, tiled=True),
        lax.all_gather(expert_down, "fs", axis=1, tiled=True),
        lax.all_gather(shared_gate_cast, "fs", axis=1, tiled=True),
        lax.all_gather(shared_up_cast, "fs", axis=1, tiled=True),
        lax.all_gather(shared_down_cast, "fs", axis=1, tiled=True),
    )
    gate_full, up_full, down_full, sgate_full, sup_full, sdown_full = gathered
    gate_pre = contract(slot_rows, gate_full[0])
    up_pre = contract(slot_rows, up_full[0])
    sgate_part = contract(normed_cols, sgate_full[0])
    sup_part = contract(normed_cols, sup_full[0])
    expert_act = (jax.nn.silu(gate_pre) * up_pre).astype(jnp.bfloat16)
    shared_gate_pre, shared_up_pre = lax.psum((sgate_part, sup_part), "tp")
    shared_act = (jax.nn.silu(shared_gate_pre) * shared_up_pre).astype(jnp.bfloat16)
    expert_out = jnp.dot(expert_act, down_full[0], preferred_element_type=jnp.float32)
    shared_out = jnp.dot(shared_act, sdown_full[0], preferred_element_type=jnp.float32)
    arrived = lax.all_to_all(expert_out, "tp", split_axis=1, concat_axis=0, tiled=True)
    arrived = arrived.reshape(expert_count, capacity, column_width)

    def add_expert(total, inputs):
        source_index, source_rows = inputs
        source_chosen = expert_ids == source_index
        source_weight = jnp.sum(jnp.where(source_chosen, route_weight, 0.0), axis=1)
        source_present = jnp.any(source_chosen, axis=1)
        source_position = jnp.cumsum(source_present.astype(jnp.int32)) - 1
        source_picked = jnp.take(source_rows, jnp.maximum(source_position, 0), axis=0)
        return (
            total + jnp.where(source_present[:, None], source_picked * source_weight[:, None], 0.0),
            None,
        )

    routed_cols, _ = lax.scan(
        add_expert,
        jnp.zeros((token_count, column_width), jnp.float32),
        (jnp.arange(expert_count, dtype=jnp.int32), arrived),
    )
    mixture = (routed_cols + shared_out).astype(jnp.bfloat16)
    return (gate_full, up_full, down_full, sgate_full[0], sup_full[0], sdown_full[0], mixture)


def solution(mesh):
    placed = (
        P(None, "fs", "tp"),
        P(None, "fs", "tp"),
        P(None, "fs", "tp"),
        P("fs", "tp"),
        P("fs", "tp"),
        P("fs", "tp"),
        P("tp"),
        P("fs", None),
        P("fs", None),
        P("fs", None),
    )
    return jax.shard_map(
        on_device,
        mesh=mesh,
        in_specs=placed,
        out_specs=(
            P("tp", None, None),
            P("tp", None, None),
            P("tp", None, None),
            P(None, "tp"),
            P(None, "tp"),
            P(None, "tp"),
            P("fs", "tp"),
        ),
        check_vma=False,
    )
```

profile of v0, /device:TPU:0, one launch (start us, length us, event | category | flops | bytes accessed | tf_op | source)
XLA Modules:
  0.0 302.3 jit_solution(17603221546341830678)
XLA Ops:
  8.0 2.5 multiply_convert_fusion
  10.9 34.5 %all_to_all.67 = bf16[16,252,128]{2,1,0:T(8,128)(2,1)S(1)} all-to-all(bf16[16,252,128]{2,1,0:T(8,128)(2,1)S(1)} %copy.55), channel_id=1, replica_groups=mesh['fs'=2,'tp'=16] {'tp'}, dimensions={0} | all-to-all | bytes 2064384 | tf_op jit(solution)/shard_map/all_to_all | solution.py:35
  45.9 3.7 %copy.57 = bf16[1,252,2048]{2,0,1:T(2,128)(2,1)} copy(bf16[1,252,2048]{1,2,0:T(8,128)(2,1)S(1)} %bitcast.74) | data formatting | bytes 2064384 | tf_op jit(solution)/shard_map/all_to_all | solution.py:35
  49.9 29.4 %all_to_all.68 = bf16[16,252,128]{2,1,0:T(8,128)(2,1)S(1)} all-to-all(bf16[16,252,128]{2,1,0:T(8,128)(2,1)S(1)} %copy.58), channel_id=1, replica_groups=mesh['fs'=2,'tp'=16] {'tp'}, dimensions={0} | all-to-all | bytes 2064384 | tf_op jit(solution)/shard_map/all_to_all | solution.py:36
  79.9 3.7 %copy.60 = bf16[1,252,2048]{2,0,1:T(2,128)(2,1)} copy(bf16[1,252,2048]{1,2,0:T(8,128)(2,1)S(1)} %bitcast.75) | data formatting | bytes 2064384 | tf_op jit(solution)/shard_map/all_to_all | solution.py:36
  83.8 1.2 copy.61
  85.1 3.9 %all-to-all-start.2 = ((bf16[16,252,128]{2,1,0:T(8,128)(2,1)}), bf16[16,252,128]{2,1,0:T(8,128)(2,1)S(1)}, u32[]{:S(2)}, u32[]{:S(2)}) async-start(bf16[16,252,128]{2,1,0:T(8,128)(2,1)} %copy.61), calls=%async_computation.2 | async-start | bytes 2097152 | tf_op jit(solution)/shard_map/all_to_all | solution.py:37
  89.6 23.0 %all-to-all-done.2 = bf16[16,252,128]{2,1,0:T(8,128)(2,1)S(1)} async-done(((bf16[16,252,128]{2,1,0:T(8,128)(2,1)}), bf16[16,252,128]{2,1,0:T(8,128)(2,1)S(1)}, u32[]{:S(2)}, u32[]{:S(2)}) %all-to-all-start.2) | async-done | bytes 1032224 | tf_op jit(solution)/shard_map/all_to_all | solution.py:37
  113.1 3.9 %copy.63 = bf16[1,252,2048]{2,0,1:T(2,128)(2,1)} copy(bf16[1,252,2048]{1,2,0:T(8,128)(2,1)S(1)} %bitcast.76) | data formatting | bytes 2064384 | tf_op jit(solution)/shard_map/all_to_all | solution.py:37
  117.9 2.3 gather_fusion.1
  120.2 3.4 %copy.66 = bf16[1,504,2048]{2,1,0:T(8,128)(2,1)S(1)} copy(bf16[1,504,2048]{2,0,1:T(2,128)(2,1)} %all-gather.10.cloned.1.call-done) | data formatting | bytes 4128768
  123.7 6.1 %copy.67 = bf16[1,504,2048]{2,1,0:T(8,128)(2,1)} copy(bf16[1,504,2048]{2,0,1:T(2,128)(2,1)} %all-gather.12.cloned.1.call-done) | data formatting | bytes 4128768
  129.8 1.6 fusion.4
  131.4 9.0 %copy.73 = bf16[1,504,2048]{1,2,0:T(8,128)(2,1)S(1)} copy(bf16[1,504,2048]{2,0,1:T(2,128)(2,1)} %all-gather.14.cloned.1.call-done) | data formatting | bytes 4128768 | tf_op jit(solution)/shard_map/dot_general | solution.py:78
  140.4 5.8 %fusion.17 = f32[256,16,128]{2,0,1:T(8,128)} fusion(bf16[16,128,504]{2,1,0:T(8,128)(2,1)S(1)} %bitcast.78, bf16[1,504,2048]{2,1,0:T(8,128)(2,1)} %copy.67, f32[256,504]{0,1:T(8,128)} %fusion.4, bf16[256,2048]{1,0:T(8,128)(2,1)} %gather_fusion.1, pred[256]{0:T(512)(128)(4,1)S(1)} %compare_and_fusion), kind=kOutput, calls=%fused_computation.27 | convolution fusion | flops 1058263040 | bytes 7790848 | tf_op jit(solution)/shard_map/dot_general | solution.py:78
  146.2 6.6 %all-to-all-start.3 = ((f32[256,16,128]{2,0,1:T(8,128)}), f32[256,16,128]{2,0,1:T(8,128)S(1)}, u32[]{:S(2)}, u32[]{:S(2)}) async-start(f32[256,16,128]{2,0,1:T(8,128)} %fusion.17), calls=%async_computation.3 | async-start | bytes 4194304 | tf_op jit(solution)/shard_map/all_to_all | solution.py:80
  153.0 1.9 all-gather.3
  154.9 1.9 all-gather.4
  159.1 2.1 all-gather.5
  161.2 4.8 %copy.68 = bf16[1,504,2048]{2,1,0:T(8,128)(2,1)} copy(bf16[1,504,2048]{2,0,1:T(2,128)(2,1)} %all-gather.14.cloned.1.call-done) | data formatting | bytes 4128768
  166.0 38.5 %all-to-all-done.3 = f32[256,16,128]{2,0,1:T(8,128)S(1)} async-done(((f32[256,16,128]{2,0,1:T(8,128)}), f32[256,16,128]{2,0,1:T(8,128)S(1)}, u32[]{:S(2)}, u32[]{:S(2)}) %all-to-all-start.3) | async-done | bytes 2097184 | tf_op jit(solution)/shard_map/all_to_all | solution.py:80
  204.4 47.8 %while.13 = (s32[]{:T(128)}, f32[256,128]{1,0:T(8,128)S(1)}, s32[16]{0:T(128)S(1)}, s32[256,8]{0,1:T(8,128)S(1)}, f32[16,256,128]{2,1,0:T(8,128)S(1)}, /*index=5...) while((s32[]{:T(128)}, f32[256,128]{1,0:T(8,128)S(1)}, s32[16]{0:T(128)S(1)}, ...), condition=%wide.region_11.12_spmd.clone, body=%wide.region_6.11_spmd.clone.sunk | while | flops 206342 | bytes 952776 | solution.py:95
  252.2 40.8 %all-reduce.3.cloned.1.call-done = (f32[256,504]{0,1:T(8,128)}, f32[256,504]{0,1:T(8,128)}) async-done(((f32[256,504]{0,1:T(8,128)}, f32[256,504]{0,1:T(8,128)}), (f32[256,504]{0,1:T(8,128)}, f32[256,504]{0,1:T(8,128)})) %all-reduce.3.cloned.1.call-update) | async-done | bytes 1032208 | tf_op jit(solution)/shard_map/psum | solution.py:76
  293.0 2.2 fusion.15
  (276 shorter events, 53.3 us)
Async XLA Ops:
  8.0 112.2 %all-gather.10.cloned.1.call-start = ((), (), s32[]{:S(2)}) async-start(), calls=%async_computation.4 | async-start | bytes 6193152 | tf_op jit(solution)/shard_map/all_gather | solution.py:63
  49.6 74.1 %all-gather.12.cloned.1.call-start = ((), (), s32[]{:S(2)}) async-start(), calls=%async_computation.5 | async-start | bytes 6193152 | tf_op jit(solution)/shard_map/all_gather | solution.py:64
  79.9 3.8 %copy-start.2 = (f32[16,252,128]{2,0,1:T(8,128)S(1)}, f32[16,252,128]{2,0,1:T(8,128)}, u32[]{:S(2)}) copy-start(f32[16,252,128]{2,0,1:T(8,128)} %param.14) | copy-start | bytes 6193156
  83.8 5.2 %copy-start.6 = (s32[256,8]{0,1:T(8,128)S(1)}, s32[256,8]{0,1:T(8,128)}, u32[]{:S(2)}) copy-start(s32[256,8]{0,1:T(8,128)} %param.20) | copy-start | bytes 24580
  85.1 27.5 %all-to-all-start.2 = ((bf16[16,252,128]{2,1,0:T(8,128)(2,1)}), bf16[16,252,128]{2,1,0:T(8,128)(2,1)S(1)}, u32[]{:S(2)}, u32[]{:S(2)}) async-start(bf16[16,252,128]{2,1,0:T(8,128)(2,1)} %copy.61), calls=%async_computation.2 | async-start | bytes 2097152 | tf_op jit(solution)/shard_map/all_to_all | solution.py:37
  89.0 42.4 %all-gather.14.cloned.1.call-start = ((), (), s32[]{:S(2)}) async-start(), calls=%async_computation.6 | async-start | bytes 6193152 | tf_op jit(solution)/shard_map/all_gather | solution.py:65
  113.1 4.2 %copy-start = (bf16[256,2048]{1,0:T(8,128)(2,1)S(1)}, bf16[256,2048]{1,0:T(8,128)(2,1)}, u32[]{:S(2)}) copy-start(bf16[256,2048]{1,0:T(8,128)(2,1)} %param.19) | copy-start | bytes 3145732
  123.6 6.1 %copy-start.1 = (bf16[1,504,2048]{2,1,0:T(8,128)(2,1)}, bf16[1,504,2048]{2,1,0:T(8,128)(2,1)S(1)}, u32[]{:S(2)}) copy-start(bf16[1,504,2048]{2,1,0:T(8,128)(2,1)S(1)} %copy.66) | copy-start | bytes 6193156
  123.7 6.1 %copy-start.3 = (bf16[256,2048]{1,0:T(8,128)(2,1)S(1)}, bf16[256,2048]{1,0:T(8,128)(2,1)}, u32[]{:S(2)}) copy-start(bf16[256,2048]{1,0:T(8,128)(2,1)} %gather_fusion.1) | copy-start | bytes 3145732
  146.2 6.7 %copy-start.8 = (f32[252,128]{1,0:T(8,128)S(1)}, f32[252,128]{1,0:T(8,128)}, u32[]{:S(2)}) copy-start(f32[252,128]{1,0:T(8,128)} %param.16) | copy-start | bytes 387076
  146.2 6.7 %copy-start.9 = (f32[252,128]{1,0:T(8,128)S(1)}, f32[252,128]{1,0:T(8,128)}, u32[]{:S(2)}) copy-start(f32[252,128]{1,0:T(8,128)} %param.15) | copy-start | bytes 387076
  146.2 6.7 %copy-start.12 = (f32[128]{0:T(128)S(1)}, f32[128]{0:T(128)}, u32[]{:S(2)}) copy-start(f32[128]{0:T(128)} %param.18) | copy-start | bytes 1540
  146.2 58.2 %all-to-all-start.3 = ((f32[256,16,128]{2,0,1:T(8,128)}), f32[256,16,128]{2,0,1:T(8,128)S(1)}, u32[]{:S(2)}, u32[]{:S(2)}) async-start(f32[256,16,128]{2,0,1:T(8,128)} %fusion.17), calls=%async_computation.3 | async-start | bytes 4194304 | tf_op jit(solution)/shard_map/all_to_all | solution.py:80
  152.8 140.2 %all-reduce.3.cloned.1.call-start = ((), (), s32[]{:S(2)}) async-start(), calls=%async_computation.7 | async-start | bytes 2064384 | tf_op jit(solution)/shard_map/psum | solution.py:76
  152.9 8.2 %copy-start.11 = (f32[256,8]{0,1:T(8,128)S(1)}, f32[256,8]{0,1:T(8,128)}, u32[]{:S(2)}) copy-start(f32[256,8]{0,1:T(8,128)} %param.21) | copy-start | bytes 24580
  154.9 11.1 %copy-start.4 = (bf16[504,128]{1,0:T(8,128)(2,1)}, bf16[504,128]{1,0:T(8,128)(2,1)S(1)}, u32[]{:S(2)}) copy-start(bf16[504,128]{1,0:T(8,128)(2,1)S(1)} %reshape.181) | copy-start | bytes 387076
  156.8 9.1 %copy-start.5 = (bf16[504,128]{1,0:T(8,128)(2,1)}, bf16[504,128]{1,0:T(8,128)(2,1)S(1)}, u32[]{:S(2)}) copy-start(bf16[504,128]{1,0:T(8,128)(2,1)S(1)} %reshape.183) | copy-start | bytes 387076
  156.8 2.2 copy-start.7
  161.2 131.8 %copy-start.10 = (bf16[504,128]{1,0:T(8,128)(2,1)}, bf16[504,128]{1,0:T(8,128)(2,1)S(1)}, u32[]{:S(2)}) copy-start(bf16[504,128]{1,0:T(8,128)(2,1)S(1)} %reshape.185) | copy-start | bytes 387076
Sparse Core Ops, SparseCore 0:
  49.7 11.8 all-gather.9
  83.8 11.8 all-gather.11
  117.2 13.8 all-gather.13
Sparse Core Ops, SparseCore 1:
  159.1 133.8 all-reduce.2
where the time goes:
time: 303 us; the launch traced here: 302 us
  waiting for transfers between devices  102 us (34%)
  blocking collectives  69.7 us (23%)
  local copies, waits for them, and re-layouts  66.4 us (22%)
  other arithmetic  25.3 us (8%)
  between operations  15.5 us (5%)
  matrix products  11.7 us (4%)
  starting transfers between devices  10.7 us (4%)
    psum x1, waiting for transfers between devices, on_device(): shared_gate_pre, shared_up_pre = lax.psum((sgate_part, sup_part), 'tp')  40.8 us
    all_to_all x1, waiting for transfers between devices, on_device(): lax.all_to_all(expert_out, 'tp', split_axis=1, concat_axis=0, tiled=True)  38.5 us
    all_to_all x1, blocking collectives, on_device(): lax.all_to_all(gate_cast, 'tp', split_axis=0, concat_axis=2, tiled=True)  34.5 us
    all_to_all x1, blocking collectives, on_device(): lax.all_to_all(up_cast, 'tp', split_axis=0, concat_axis=2, tiled=True)  29.4 us
    all_to_all x1, waiting for transfers between devices, on_device(): lax.all_to_all(down_cast, 'tp', split_axis=0, concat_axis=2, tiled=True)  23 us
    unnamed x32, local copies, waits for them, and re-layouts  14.4 us
    gather x16, local copies, waits for them, and re-layouts, add_expert(): jnp.take(source_rows, jnp.maximum(source_position, 0), axis=0)  11.7 us
    reduce_sum x16, other arithmetic, add_expert(): source_weight = jnp.sum(jnp.where(source_chosen, route_weight, 0.0), axis=1)  11.3 us
  transfers between devices with their start and end apart: 6, of which 3 were waited for; matrix products, arithmetic and copies ran while one was open for 26% of the time, Pallas kernels for 0%

commit v1 on v0

--- a/solution.py
+++ b/solution.py
@@ -5,6 +5,22 @@
 
 EPSILON = 1e-06
 ROUTED_SCALE = 2.5
+
+
+def swapped_with_each(x, axis, split, join):
+    ways, here = (lax.axis_size(axis), lax.axis_index(axis))
+    width = x.shape[split] // ways
+    dims = list(x.shape)
+    dims[split] = width
+    height = dims[join]
+    dims[join] = height * ways
+    full = jnp.zeros(dims, x.dtype)
+    for mask in range(ways):
+        part = lax.dynamic_slice_in_dim(x, (here ^ mask) * width, width, axis=split)
+        if mask:
+            part = lax.ppermute(part, axis, [(d, d ^ mask) for d in range(ways)])
+        full = lax.dynamic_update_slice_in_dim(full, part, (here ^ mask) * height, axis=join)
+    return full
 
 
 def contract(left, right):
@@ -32,7 +48,7 @@
     shared_up_cast = (trained_shared_up * ffn_gain[None, :]).astype(jnp.bfloat16)[None]
     shared_down_cast = trained_shared_down.astype(jnp.bfloat16)[None]
     expert_gate, expert_up, expert_down = (
-        lax.all_to_all(gate_cast, "tp", split_axis=0, concat_axis=2, tiled=True),
+        swapped_with_each(gate_cast, "tp", 0, 2),
         lax.all_to_all(up_cast, "tp", split_axis=0, concat_axis=2, tiled=True),
         lax.all_to_all(down_cast, "tp", split_axis=0, concat_axis=2, tiled=True),
     )

time: 303 us -> 332 us (1.096)
  starting transfers between devices: 10.7 us -> 45.8 us
  blocking collectives: 69.7 us -> 41.3 us
  waiting for transfers between devices: 102 us -> 117 us
  local copies, waits for them, and re-layouts: 66.4 us -> 74.5 us
    ppermute x0 -> x15, starting transfers between devices: none -> 34.9 us  [swapped_with_each(): part = lax.ppermute(part, axis, [(d, d ^ mask) for d in range(ways)])]
    all_to_all x1 -> x0, blocking collectives: 34.5 us -> none  [on_device(): lax.all_to_all(gate_cast, 'tp', split_axis=0, concat_axis=2, tiled=True)]
    ppermute x0 -> x15, waiting for transfers between devices: none -> 12.7 us  [swapped_with_each(): part = lax.ppermute(part, axis, [(d, d ^ mask) for d in range(ways)])]
    dynamic_update_slice x0 -> x15, local copies, waits for them, and re-layouts: none -> 7.86 us  [swapped_with_each(): lax.dynamic_update_slice_in_dim(full, part, (here ^ mask) * height, axis=...]
    all_to_all x1, blocking collectives: 29.4 us -> 35.6 us  [on_device(): lax.all_to_all(up_cast, 'tp', split_axis=0, concat_axis=2, tiled=True)]
    all_to_all x2 -> x0, local copies, waits for them, and re-layouts: 4.26 us -> none  [on_device(): lax.all_to_all(gate_cast, 'tp', split_axis=0, concat_axis=2, tiled=True)]
    unnamed x32 -> x34, local copies, waits for them, and re-layouts: 14.4 us -> 16.6 us
  transfers between devices with their start and end apart: 6 -> 21, of which waited for: 3 -> 7; matrix products, arithmetic and copies ran while one was open for 26% -> 25% of each run, Pallas kernels for 0% -> 0%
where the time goes in v1:
time: 332 us; the launch traced here: 331 us
  waiting for transfers between devices  117 us (35%)
  local copies, waits for them, and re-layouts  74.5 us (22%)
  starting transfers between devices  45.8 us (14%)
  blocking collectives  41.3 us (12%)
  other arithmetic  24.4 us (7%)
  between operations  15.8 us (5%)
  matrix products  11.8 us (4%)
    psum x1, waiting for transfers between devices, on_device(): shared_gate_pre, shared_up_pre = lax.psum((sgate_part, sup_part), 'tp')  42.6 us
    all_to_all x1, waiting for transfers between devices, on_device(): lax.all_to_all(expert_out, 'tp', split_axis=1, concat_axis=0, tiled=True)  38.6 us
    all_to_all x1, blocking collectives, on_device(): lax.all_to_all(up_cast, 'tp', split_axis=0, concat_axis=2, tiled=True)  35.6 us
    ppermute x15, starting transfers between devices, swapped_with_each(): part = lax.ppermute(part, axis, [(d, d ^ mask) for d in range(ways)])  34.9 us
    all_to_all x1, waiting for transfers between devices, on_device(): lax.all_to_all(down_cast, 'tp', split_axis=0, concat_axis=2, tiled=True)  22.6 us
    unnamed x34, local copies, waits for them, and re-layouts  16.6 us
    ppermute x15, waiting for transfers between devices, swapped_with_each(): part = lax.ppermute(part, axis, [(d, d ^ mask) for d in range(ways)])  12.7 us
    gather x16, local copies, waits for them, and re-layouts, add_expert(): jnp.take(source_rows, jnp.maximum(source_position, 0), axis=0)  11.7 us
  transfers between devices with their start and end apart: 21, of which 7 were waited for; matrix products, arithmetic and copies ran while one was open for 25% of the time, Pallas kernels for 0%

profile of v1, /device:TPU:0, one launch (start us, length us, event | category | flops | bytes accessed | tf_op | source)
XLA Modules:
  0.0 330.8 jit_solution(9658037919233512335)
XLA Ops:
  8.2 2.5 multiply_convert_fusion
  11.8 3.3 constant_dynamic-slice_fusion
  15.1 3.0 collective-permute-start
  23.0 2.5 collective-permute-start.5
  29.4 2.6 collective-permute-start.7
  41.5 3.1 collective-permute-start.11
  44.8 7.1 %collective-permute-done.7 = bf16[1,252,128]{2,0,1:T(2,128)(2,1)S(1)} collective-permute-done((bf16[1,252,128]{2,0,1:T(2,128)(2,1)}, bf16[1,252,128]{2,0,1:T(2,128)(2,1)S(1)}, u32[]{:S(2)}, u32[]{:S(2)}) %collective-permute-start.7) | collective-permute-done | bytes 64544 | tf_op jit(solution)/shard_map/ppermute | solution.py:21
  51.9 2.6 collective-permute-start.12
  58.3 2.9 collective-permute-done.9
  61.1 6.3 %collective-permute-start.14 = (bf16[1,252,128]{2,0,1:T(2,128)(2,1)S(1)}, bf16[1,252,128]{2,0,1:T(2,128)(2,1)S(1)}, u32[]{:S(2)}, u32[]{:S(2)}) collective-permute-start(bf16[1,252,128]{2,0,1:T(2,128)(2,1)S(1)} %get-tuple-element.166), channel_id=1, source_target_pairs={{0,15},{1,14},{2,13},{3,12},{4,11},{5,10},{6,9},{7,8},{8,7},{9,6},... | collective-permute-start | bytes 193544 | tf_op jit(solution)/shard_map/ppermute | solution.py:21
  72.4 35.6 %all_to_all.49 = bf16[16,252,128]{2,1,0:T(8,128)(2,1)S(1)} all-to-all(bf16[16,252,128]{2,1,0:T(8,128)(2,1)S(1)} %copy.72), channel_id=1, replica_groups=mesh['fs'=2,'tp'=16] {'tp'}, dimensions={0} | all-to-all | bytes 2064384 | tf_op jit(solution)/shard_map/all_to_all | solution.py:52
  108.5 3.7 %copy.74 = bf16[1,252,2048]{2,0,1:T(2,128)(2,1)} copy(bf16[1,252,2048]{1,2,0:T(8,128)(2,1)S(1)} %bitcast.67) | data formatting | bytes 2064384 | tf_op jit(solution)/shard_map/all_to_all | solution.py:52
  113.7 3.8 %all-to-all-start.1 = ((bf16[16,252,128]{2,1,0:T(8,128)(2,1)}), bf16[16,252,128]{2,1,0:T(8,128)(2,1)S(1)}, u32[]{:S(2)}, u32[]{:S(2)}) async-start(bf16[16,252,128]{2,1,0:T(8,128)(2,1)} %copy.75), calls=%async_computation.1 | async-start | bytes 2097152 | tf_op jit(solution)/shard_map/all_to_all | solution.py:53
  118.3 22.6 %all-to-all-done.1 = bf16[16,252,128]{2,1,0:T(8,128)(2,1)S(1)} async-done(((bf16[16,252,128]{2,1,0:T(8,128)(2,1)}), bf16[16,252,128]{2,1,0:T(8,128)(2,1)S(1)}, u32[]{:S(2)}, u32[]{:S(2)}) %all-to-all-start.1) | async-done | bytes 1032224 | tf_op jit(solution)/shard_map/all_to_all | solution.py:53
  141.5 3.9 %copy.77 = bf16[1,252,2048]{2,0,1:T(2,128)(2,1)} copy(bf16[1,252,2048]{1,2,0:T(8,128)(2,1)S(1)} %bitcast.68) | data formatting | bytes 2064384 | tf_op jit(solution)/shard_map/all_to_all | solution.py:53
  147.7 5.1 %copy.80 = bf16[1,504,2048]{2,1,0:T(8,128)(2,1)} copy(bf16[1,504,2048]{2,0,1:T(2,128)(2,1)} %all-gather.10.cloned.1.call-done) | data formatting | bytes 4128768
  152.7 4.1 %copy.81 = bf16[1,504,2048]{2,1,0:T(8,128)(2,1)S(1)} copy(bf16[1,504,2048]{2,0,1:T(2,128)(2,1)} %all-gather.12.cloned.1.call-done) | data formatting | bytes 4128768
  159.7 9.0 %copy.87 = bf16[1,504,2048]{1,2,0:T(8,128)(2,1)S(1)} copy(bf16[1,504,2048]{2,0,1:T(2,128)(2,1)} %all-gather.14.cloned.1.call-done) | data formatting | bytes 4128768 | tf_op jit(solution)/shard_map/dot_general | solution.py:94
  168.7 5.8 %fusion.13 = f32[256,16,128]{2,0,1:T(8,128)} fusion(bf16[16,128,504]{2,1,0:T(8,128)(2,1)S(1)} %bitcast.70, f32[256,504]{0,1:T(8,128)} %fusion.2, bf16[1,504,2048]{2,1,0:T(8,128)(2,1)} %copy.80, bf16[256,2048]{1,0:T(8,128)(2,1)} %copy-done.4, pred[256]{0:T(512)(128)(4,1)S(1)} %compare_and_fusion), kind=kOutput, calls=%fused_computation.27 | convolution fusion | flops 1058263040 | bytes 7790848 | tf_op jit(solution)/shard_map/dot_general | solution.py:94
  174.6 6.6 %all-to-all-start.2 = ((f32[256,16,128]{2,0,1:T(8,128)}), f32[256,16,128]{2,0,1:T(8,128)S(1)}, u32[]{:S(2)}, u32[]{:S(2)}) async-start(f32[256,16,128]{2,0,1:T(8,128)} %fusion.13), calls=%async_computation.2 | async-start | bytes 4194304 | tf_op jit(solution)/shard_map/all_to_all | solution.py:96
  189.5 4.8 %copy.82 = bf16[1,504,2048]{2,1,0:T(8,128)(2,1)} copy(bf16[1,504,2048]{2,0,1:T(2,128)(2,1)} %all-gather.14.cloned.1.call-done) | data formatting | bytes 4128768
  194.2 38.6 %all-to-all-done.2 = f32[256,16,128]{2,0,1:T(8,128)S(1)} async-done(((f32[256,16,128]{2,0,1:T(8,128)}), f32[256,16,128]{2,0,1:T(8,128)S(1)}, u32[]{:S(2)}, u32[]{:S(2)}) %all-to-all-start.2) | async-done | bytes 2097184 | tf_op jit(solution)/shard_map/all_to_all | solution.py:96
  232.8 46.1 %while.13 = (s32[]{:T(128)}, f32[256,128]{1,0:T(8,128)S(1)}, s32[16]{0:T(128)S(1)}, s32[256,8]{0,1:T(8,128)S(1)}, f32[16,256,128]{2,1,0:T(8,128)S(1)}, /*index=5...) while((s32[]{:T(128)}, f32[256,128]{1,0:T(8,128)S(1)}, s32[16]{0:T(128)S(1)}, ...), condition=%wide.region_11.12_spmd.clone, body=%wide.region_6.11_spmd.clone.sunk | while | flops 206342 | bytes 952776 | solution.py:111
  278.9 42.6 %all-reduce.3.cloned.1.call-done = (f32[256,504]{0,1:T(8,128)}, f32[256,504]{0,1:T(8,128)}) async-done(((f32[256,504]{0,1:T(8,128)}, f32[256,504]{0,1:T(8,128)}), (f32[256,504]{0,1:T(8,128)}, f32[256,504]{0,1:T(8,128)})) %all-reduce.3.cloned.1.call-update) | async-done | bytes 1032208 | tf_op jit(solution)/shard_map/psum | solution.py:92
  (321 shorter events, 92.2 us)
Async XLA Ops:
  8.0 139.6 %all-gather.10.cloned.1.call-start = ((), (), s32[]{:S(2)}) async-start(), calls=%async_computation.3 | async-start | bytes 6193152 | tf_op jit(solution)/shard_map/all_gather | solution.py:79
  15.1 7.9 %collective-permute-start = (bf16[1,252,128]{2,0,1:T(2,128)(2,1)}, bf16[1,252,128]{2,0,1:T(2,128)(2,1)}, u32[]{:S(2)}, u32[]{:S(2)}) collective-permute-start(bf16[1,252,128]{2,0,1:T(2,128)(2,1)} %get-tuple-element.180), channel_id=1, source_target_pairs={{0,1},{1,0},{2,3},{3,2},{4,5},{5,4},{6,7},{7,6},{8,9},{9,8},{10,11... | collective-permute-start | bytes 193544 | tf_op jit(solution)/shard_map/ppermute | solution.py:21
  18.0 8.6 %collective-permute-start.1 = (bf16[1,252,128]{2,0,1:T(2,128)(2,1)}, bf16[1,252,128]{2,0,1:T(2,128)(2,1)}, u32[]{:S(2)}, u32[]{:S(2)}) collective-permute-start(bf16[1,252,128]{2,0,1:T(2,128)(2,1)} %get-tuple-element.179), channel_id=1, source_target_pairs={{0,2},{1,3},{2,0},{3,1},{4,6},{5,7},{6,4},{7,5},{8,10},{9,11},{10,... | collective-permute-start | bytes 193544 | tf_op jit(solution)/shard_map/ppermute | solution.py:21
  19.5 9.8 %collective-permute-start.2 = (bf16[1,252,128]{2,0,1:T(2,128)(2,1)}, bf16[1,252,128]{2,0,1:T(2,128)(2,1)}, u32[]{:S(2)}, u32[]{:S(2)}) collective-permute-start(bf16[1,252,128]{2,0,1:T(2,128)(2,1)} %get-tuple-element.178), channel_id=1, source_target_pairs={{0,3},{1,2},{2,1},{3,0},{4,7},{5,6},{6,5},{7,4},{8,11},{9,10},{10,... | collective-permute-start | bytes 193544 | tf_op jit(solution)/shard_map/ppermute | solution.py:21
  19.5 13.6 %collective-permute-start.3 = (bf16[1,252,128]{2,0,1:T(2,128)(2,1)}, bf16[1,252,128]{2,0,1:T(2,128)(2,1)}, u32[]{:S(2)}, u32[]{:S(2)}) collective-permute-start(bf16[1,252,128]{2,0,1:T(2,128)(2,1)} %get-tuple-element.177), channel_id=1, source_target_pairs={{0,4},{1,5},{2,6},{3,7},{4,0},{5,1},{6,2},{7,3},{8,12},{9,13},{10,... | collective-permute-start | bytes 193544 | tf_op jit(solution)/shard_map/ppermute | solution.py:21
  21.6 14.9 %collective-permute-start.4 = (bf16[1,252,128]{2,0,1:T(2,128)(2,1)}, bf16[1,252,128]{2,0,1:T(2,128)(2,1)}, u32[]{:S(2)}, u32[]{:S(2)}) collective-permute-start(bf16[1,252,128]{2,0,1:T(2,128)(2,1)} %get-tuple-element.176), channel_id=1, source_target_pairs={{0,5},{1,4},{2,7},{3,6},{4,1},{5,0},{6,3},{7,2},{8,13},{9,12},{10,... | collective-permute-start | bytes 193544 | tf_op jit(solution)/shard_map/ppermute | solution.py:21
  23.0 16.2 %collective-permute-start.5 = (bf16[1,252,128]{2,0,1:T(2,128)(2,1)}, bf16[1,252,128]{2,0,1:T(2,128)(2,1)S(1)}, u32[]{:S(2)}, u32[]{:S(2)}) collective-permute-start(bf16[1,252,128]{2,0,1:T(2,128)(2,1)} %get-tuple-element.175), channel_id=1, source_target_pairs={{0,6},{1,7},{2,4},{3,5},{4,2},{5,3},{6,0},{7,1},{8,14},{9,15},{10,... | collective-permute-start | bytes 193544 | tf_op jit(solution)/shard_map/ppermute | solution.py:21
  26.6 14.9 %collective-permute-start.6 = (bf16[1,252,128]{2,0,1:T(2,128)(2,1)}, bf16[1,252,128]{2,0,1:T(2,128)(2,1)S(1)}, u32[]{:S(2)}, u32[]{:S(2)}) collective-permute-start(bf16[1,252,128]{2,0,1:T(2,128)(2,1)} %get-tuple-element.174), channel_id=1, source_target_pairs={{0,7},{1,6},{2,5},{3,4},{4,3},{5,2},{6,1},{7,0},{8,15},{9,14},{10,... | collective-permute-start | bytes 193544 | tf_op jit(solution)/shard_map/ppermute | solution.py:21
  29.4 22.5 %collective-permute-start.7 = (bf16[1,252,128]{2,0,1:T(2,128)(2,1)}, bf16[1,252,128]{2,0,1:T(2,128)(2,1)S(1)}, u32[]{:S(2)}, u32[]{:S(2)}) collective-permute-start(bf16[1,252,128]{2,0,1:T(2,128)(2,1)} %get-tuple-element.173), channel_id=1, source_target_pairs={{0,8},{1,9},{2,10},{3,11},{4,12},{5,13},{6,14},{7,15},{8,0},{9,1},... | collective-permute-start | bytes 193544 | tf_op jit(solution)/shard_map/ppermute | solution.py:21
  33.1 22.5 %collective-permute-start.8 = (bf16[1,252,128]{2,0,1:T(2,128)(2,1)}, bf16[1,252,128]{2,0,1:T(2,128)(2,1)S(1)}, u32[]{:S(2)}, u32[]{:S(2)}) collective-permute-start(bf16[1,252,128]{2,0,1:T(2,128)(2,1)} %get-tuple-element.172), channel_id=1, source_target_pairs={{0,9},{1,8},{2,11},{3,10},{4,13},{5,12},{6,15},{7,14},{8,1},{9,0},... | collective-permute-start | bytes 193544 | tf_op jit(solution)/shard_map/ppermute | solution.py:21
  36.5 24.6 %collective-permute-start.9 = (bf16[1,252,128]{2,0,1:T(2,128)(2,1)}, bf16[1,252,128]{2,0,1:T(2,128)(2,1)S(1)}, u32[]{:S(2)}, u32[]{:S(2)}) collective-permute-start(bf16[1,252,128]{2,0,1:T(2,128)(2,1)} %get-tuple-element.171), channel_id=1, source_target_pairs={{0,10},{1,11},{2,8},{3,9},{4,14},{5,15},{6,12},{7,13},{8,2},{9,3},... | collective-permute-start | bytes 193544 | tf_op jit(solution)/shard_map/ppermute | solution.py:21
  39.2 28.5 %collective-permute-start.10 = (bf16[1,252,128]{2,0,1:T(2,128)(2,1)}, bf16[1,252,128]{2,0,1:T(2,128)(2,1)S(1)}, u32[]{:S(2)}, u32[]{:S(2)}) collective-permute-start(bf16[1,252,128]{2,0,1:T(2,128)(2,1)} %get-tuple-element.170), channel_id=1, source_target_pairs={{0,11},{1,10},{2,9},{3,8},{4,15},{5,14},{6,13},{7,12},{8,3},{9,2},... | collective-permute-start | bytes 193544 | tf_op jit(solution)/shard_map/ppermute | solution.py:21
  41.5 26.4 %collective-permute-start.11 = (bf16[1,252,128]{2,0,1:T(2,128)(2,1)}, bf16[1,252,128]{2,0,1:T(2,128)(2,1)S(1)}, u32[]{:S(2)}, u32[]{:S(2)}) collective-permute-start(bf16[1,252,128]{2,0,1:T(2,128)(2,1)} %get-tuple-element.169), channel_id=1, source_target_pairs={{0,12},{1,13},{2,14},{3,15},{4,8},{5,9},{6,10},{7,11},{8,4},{9,5},... | collective-permute-start | bytes 193544 | tf_op jit(solution)/shard_map/ppermute | solution.py:21
  51.9 16.3 %collective-permute-start.12 = (bf16[1,252,128]{2,0,1:T(2,128)(2,1)S(1)}, bf16[1,252,128]{2,0,1:T(2,128)(2,1)S(1)}, u32[]{:S(2)}, u32[]{:S(2)}) collective-permute-start(bf16[1,252,128]{2,0,1:T(2,128)(2,1)S(1)} %get-tuple-element.168), channel_id=1, source_target_pairs={{0,13},{1,12},{2,15},{3,14},{4,9},{5,8},{6,11},{7,10},{8,5},{9,4},... | collective-permute-start | bytes 193544 | tf_op jit(solution)/shard_map/ppermute | solution.py:21
  55.6 12.8 %collective-permute-start.13 = (bf16[1,252,128]{2,0,1:T(2,128)(2,1)S(1)}, bf16[1,252,128]{2,0,1:T(2,128)(2,1)S(1)}, u32[]{:S(2)}, u32[]{:S(2)}) collective-permute-start(bf16[1,252,128]{2,0,1:T(2,128)(2,1)S(1)} %get-tuple-element.167), channel_id=1, source_target_pairs={{0,14},{1,15},{2,12},{3,13},{4,10},{5,11},{6,8},{7,9},{8,6},{9,7},... | collective-permute-start | bytes 193544 | tf_op jit(solution)/shard_map/ppermute | solution.py:21
  61.1 9.4 %collective-permute-start.14 = (bf16[1,252,128]{2,0,1:T(2,128)(2,1)S(1)}, bf16[1,252,128]{2,0,1:T(2,128)(2,1)S(1)}, u32[]{:S(2)}, u32[]{:S(2)}) collective-permute-start(bf16[1,252,128]{2,0,1:T(2,128)(2,1)S(1)} %get-tuple-element.166), channel_id=1, source_target_pairs={{0,15},{1,14},{2,13},{3,12},{4,11},{5,10},{6,9},{7,8},{8,7},{9,6},... | collective-permute-start | bytes 193544 | tf_op jit(solution)/shard_map/ppermute | solution.py:21
  72.0 80.7 %all-gather.12.cloned.1.call-start = ((), (), s32[]{:S(2)}) async-start(), calls=%async_computation.4 | async-start | bytes 6193152 | tf_op jit(solution)/shard_map/all_gather | solution.py:80
  113.7 27.3 %all-to-all-start.1 = ((bf16[16,252,128]{2,1,0:T(8,128)(2,1)}), bf16[16,252,128]{2,1,0:T(8,128)(2,1)S(1)}, u32[]{:S(2)}, u32[]{:S(2)}) async-start(bf16[16,252,128]{2,1,0:T(8,128)(2,1)} %copy.75), calls=%async_computation.1 | async-start | bytes 2097152 | tf_op jit(solution)/shard_map/all_to_all | solution.py:53
  117.5 42.2 %all-gather.14.cloned.1.call-start = ((), (), s32[]{:S(2)}) async-start(), calls=%async_computation.5 | async-start | bytes 6193152 | tf_op jit(solution)/shard_map/all_gather | solution.py:81
  147.6 9.2 %copy-start.4 = (bf16[256,2048]{1,0:T(8,128)(2,1)}, bf16[256,2048]{1,0:T(8,128)(2,1)S(1)}, u32[]{:S(2)}) copy-start(bf16[256,2048]{1,0:T(8,128)(2,1)S(1)} %gather_fusion.1) | copy-start | bytes 3145732
  174.6 58.3 %all-to-all-start.2 = ((f32[256,16,128]{2,0,1:T(8,128)}), f32[256,16,128]{2,0,1:T(8,128)S(1)}, u32[]{:S(2)}, u32[]{:S(2)}) async-start(f32[256,16,128]{2,0,1:T(8,128)} %fusion.13), calls=%async_computation.2 | async-start | bytes 4194304 | tf_op jit(solution)/shard_map/all_to_all | solution.py:96
  181.2 140.3 %all-reduce.3.cloned.1.call-start = ((), (), s32[]{:S(2)}) async-start(), calls=%async_computation.6 | async-start | bytes 2064384 | tf_op jit(solution)/shard_map/psum | solution.py:92
  183.3 10.9 %copy-start.5 = (bf16[504,128]{1,0:T(8,128)(2,1)}, bf16[504,128]{1,0:T(8,128)(2,1)S(1)}, u32[]{:S(2)}) copy-start(bf16[504,128]{1,0:T(8,128)(2,1)S(1)} %reshape.181) | copy-start | bytes 387076
  189.4 132.1 %copy-start.11 = (bf16[504,128]{1,0:T(8,128)(2,1)}, bf16[504,128]{1,0:T(8,128)(2,1)S(1)}, u32[]{:S(2)}) copy-start(bf16[504,128]{1,0:T(8,128)(2,1)S(1)} %reshape.185) | copy-start | bytes 387076
  (11 other events, 55.4 us)
Sparse Core Ops, SparseCore 0:
  72.2 18.2 all-gather.9
  112.4 11.7 all-gather.11
  145.6 13.8 all-gather.13
Sparse Core Ops, SparseCore 1:
  187.5 133.9 all-reduce.2
